TPU v7x, 32 devices: a whole 2x2x4 slice. The times are simulated.
32 devices in a mesh: kv: 8 (over z, y), tp: 4 (over x, core).
Axes of the slice: x: 2, y: 2, z: 4, core: 2. Of those that a mesh axis runs over, the one named last changes fastest.
Arguments:
- tokens: bfloat16 [64, 4096], P(None, 'kv'), may hold values from -170 to 170
- mix_gain: float32 [4096], P('kv'), may hold values from 0.1 to 1.9
- w_query: bfloat16 [4096, 2048], P('kv', 'tp'), may hold values from -0.09375 to 0.09375
- w_key: bfloat16 [4096, 512], P('kv', 'tp'), may hold values from -0.09375 to 0.09375
- w_value: bfloat16 [4096, 512], P('kv', 'tp'), may hold values from -0.09375 to 0.09375
- w_forget: bfloat16 [4096, 32], P('kv', 'tp'), may hold values from -0.09375 to 0.09375
- query_gain: float32 [64], replicated, may hold values from 0.1 to 1.9
- key_cache: bfloat16 [64, 8, 64, 8192], P(None, 'tp', None, 'kv'), may hold values from -1300 to 1300
- value_cache: bfloat16 [64, 8, 64, 8192], P(None, 'tp', None, 'kv'), may hold values from -8 to 8
- decay_cache: float32 [64, 32, 8192], P(None, 'tp', 'kv'), may hold values from -1066.96 to 0, as said below
- w_out: bfloat16 [2048, 4096], P('tp', 'kv'), may hold values from -1 to 1
- mlp_gain: float32 [4096], P('kv'), may hold values from 0.1 to 1.9
- w_up: bfloat16 [4096, 16384], P('kv', 'tp'), may hold values from -0.09375 to 0.09375
- w_down: bfloat16 [16384, 4096], P('tp', 'kv'), may hold values from -0.046875 to 0.046875
Outputs:
- layer_out: bfloat16 [64, 4096], P(None, 'kv')
Inputs may be any that keep to these rules, and one draw needn't show every extreme that they name: `decay_cache`: each entry is the sum of the non-positive log forget gates of the later cached positions of its sequence and head: 0 at the last cached position, never smaller at a later position.
All inputs are finite; a program needn't handle non-finite values.
Results may differ from a plain program's by a relative error of at most 0.015.
Values may be sent and summed in bfloat16 or wider, within the bound.
A program may use at most 128 MiB of HBM per device.

v0:
```python
import jax
import jax.numpy as jnp
from jax import lax
from jax.sharding import PartitionSpec as P

D = 4096
HEAD_DIM = 64
EPS = 1e-06


def shards(
    tokens,
    mix_gain,
    w_query,
    w_key,
    w_value,
    w_forget,
    query_gain,
    key_cache,
    value_cache,
    decay_cache,
    w_out,
    mlp_gain,
    w_up,
    w_down,
):
    row_count = tokens.shape[0]
    local_heads = w_forget.shape[1]
    local_groups = key_cache.shape[1]
    sharing = local_heads // local_groups
    score_scale = HEAD_DIM ** (-0.5)
    stream = tokens.astype(jnp.float32)
    squares_mix = jnp.sum(stream * stream, axis=1)
    normed_mix = (stream * mix_gain).astype(jnp.bfloat16)
    query_terms = jnp.dot(normed_mix, w_query, preferred_element_type=jnp.float32)
    key_terms = jnp.dot(normed_mix, w_key, preferred_element_type=jnp.float32)
    value_terms = jnp.dot(normed_mix, w_value, preferred_element_type=jnp.float32)
    forget_terms = jnp.dot(normed_mix, w_forget, preferred_element_type=jnp.float32)
    query_raw, key_raw, value_raw, forget_raw, total_mix = lax.psum(
        (query_terms, key_terms, value_terms, forget_terms, squares_mix), "kv"
    )
    scale_mix = lax.rsqrt(total_mix / D + EPS)[:, None]
    heads_raw = (scale_mix * query_raw).reshape(row_count, local_heads, HEAD_DIM)
    inverse = lax.rsqrt(jnp.mean(heads_raw * heads_raw, axis=-1, keepdims=True) + EPS)
    query = (heads_raw * inverse * query_gain).astype(jnp.bfloat16)
    query = query.reshape(row_count, local_groups, sharing, HEAD_DIM)
    key_new = (scale_mix * key_raw).reshape(row_count, local_groups, HEAD_DIM).astype(jnp.bfloat16)
    value_new = (
        (scale_mix * value_raw).reshape(row_count, local_groups, HEAD_DIM).astype(jnp.bfloat16)
    )
    log_forget = jax.nn.log_sigmoid(scale_mix * forget_raw).reshape(
        row_count, local_groups, sharing
    )
    decay = decay_cache.reshape(row_count, local_groups, sharing, -1)
    scores = (
        jnp.einsum("bgjd,bgdp->bgjp", query, key_cache, preferred_element_type=jnp.float32)
        * score_scale
    )
    scores = scores + decay + log_forget[..., None]
    own_score = (
        jnp.einsum("bgjd,bgd->bgj", query, key_new, preferred_element_type=jnp.float32)
        * score_scale
    )
    local_peak = jnp.max(scores, axis=-1)
    peak_score = jnp.maximum(lax.pmax(local_peak, "kv"), own_score)
    weights = jnp.exp(scores - peak_score[..., None])
    partial_values = jnp.einsum(
        "bgjp,bgdp->bgjd",
        weights.astype(jnp.bfloat16),
        value_cache,
        preferred_element_type=jnp.float32,
    )
    mass_sum, summed = lax.psum((jnp.sum(weights, axis=-1), partial_values), "kv")
    own_weight = jnp.exp(own_score - peak_score)
    totals = mass_sum + own_weight
    own_rounded = lax.optimization_barrier(own_weight.astype(jnp.bfloat16)).astype(jnp.float32)
    summed = summed + own_rounded[..., None] * value_new.astype(jnp.float32)[:, :, None, :]
    head_output = summed / totals[..., None]
    attended = head_output.reshape(row_count, local_heads * HEAD_DIM).astype(jnp.bfloat16)
    attn_terms = jnp.dot(attended, w_out, preferred_element_type=jnp.float32)
    attn_out = lax.psum(attn_terms.astype(jnp.bfloat16), "tp")
    attn_rounded = lax.optimization_barrier(attn_out).astype(jnp.float32)
    residual = (stream + attn_rounded).astype(jnp.bfloat16)
    residual_wide = residual.astype(jnp.float32)
    squares_mlp = jnp.sum(residual_wide * residual_wide, axis=1)
    normed_mlp = (residual_wide * mlp_gain).astype(jnp.bfloat16)
    up_terms = jnp.dot(normed_mlp, w_up, preferred_element_type=jnp.float32)
    up_full, total_mlp = lax.psum((up_terms, squares_mlp), "kv")
    scale_mlp = lax.rsqrt(total_mlp / D + EPS)[:, None]
    hidden = jnp.square(jax.nn.relu(scale_mlp * up_full)).astype(jnp.bfloat16)
    down_terms = jnp.dot(hidden, w_down, preferred_element_type=jnp.float32)
    mlp_out = lax.psum(down_terms.astype(jnp.bfloat16), "tp")
    mlp_rounded = lax.optimization_barrier(mlp_out).astype(jnp.float32)
    return (residual_wide + mlp_rounded).astype(jnp.bfloat16)


def solution(mesh):
    in_specs = (
        P(None, "kv"),
        P("kv"),
        P("kv", "tp"),
        P("kv", "tp"),
        P("kv", "tp"),
        P("kv", "tp"),
        P(),
        P(None, "tp", None, "kv"),
        P(None, "tp", None, "kv"),
        P(None, "tp", "kv"),
        P("tp", "kv"),
        P("kv"),
        P("kv", "tp"),
        P("tp", "kv"),
    )
    out_specs = P(None, "kv")
    return jax.shard_map(shards, mesh=mesh, in_specs=in_specs, out_specs=out_specs, check_vma=False)
```

profile of v0, /device:TPU:0, one launch (start us, length us, event | category | flops | bytes accessed | tf_op | source)
XLA Modules:
  0.0 406.1 jit_solution(14472312958995943851)
XLA Ops:
  6.5 1.0 copy-done
  7.6 1.7 fusion.23
  9.4 1.0 fusion.8
  10.3 1.1 fusion.19
  11.4 1.0 fusion.21
  12.4 39.3 %all-reduce.1 = (f32[64]{0:T(128)S(1)}, f32[64,8]{0,1:T(8,128)S(1)}, f32[64,128]{1,0:T(8,128)S(1)}) all-reduce(f32[64]{0:T(128)S(1)} %fusion.8, f32[64,8]{0,1:T(8,128)S(1)} %fusion.21, f32[64,128]{1,0:T(8,128)S(1)} %fusion.19), channel_id=1, replica_groups=mesh['kv'=8,'tp'=4] {'kv'}, use_global_device_ids=true, to_apply=%region_1.0 | all-reduce | flops 8768 | bytes 70144 | tf_op jit(solution)/shard_map/psum | solution.py:39
  51.9 2.0 reshape.49
  54.2 29.6 %all-reduce.8.cloned.1.call-done = f32[64,512]{1,0:T(8,128)} async-done(((f32[64,512]{1,0:T(8,128)}), f32[64,512]{1,0:T(8,128)}) %all-reduce.8.cloned.1.call-update) | async-done | bytes 131088 | tf_op jit(solution)/shard_map/psum | solution.py:39
  83.8 1.0 fusion.31
  85.7 9.4 %fusion.32 = (f32[64,2,4]{2,1,0:T(2,128)S(1)}, f32[64,2,4,1024]{3,2,1,0:T(4,128)}) fusion(f32[64,2,4]{2,1,0:T(2,128)S(1)} %copy.23, f32[64,2,4,1024]{3,2,1,0:T(4,128)S(1)} %reshape.49, bf16[64,2,4,64]{3,2,1,0:T(4,128)(2,1)S(1)} %multiply_convert_fusion.2, bf16[64,2,64,1024]{3,2,1,0:T(8,128)(2,1)} %param.21), kind=kOutput, calls=%fused_computation.47 | convolution fusion | flops 69205504 | bytes 21041152 | tf_op jit(solution)/shard_map/bgjd,bgdp->bgjp/dot_general | solution.py:56
  95.1 35.9 %pmax.7 = f32[64,2,4]{2,1,0:T(2,128)S(1)} all-reduce(f32[64,2,4]{2,1,0:T(2,128)S(1)} %get-tuple-element.14), channel_id=1, replica_groups=mesh['kv'=8,'tp'=4] {'kv'}, use_global_device_ids=true, to_apply=%region_6.0 | all-reduce | flops 512 | bytes 4096 | tf_op jit(solution)/shard_map/pmax | solution.py:65
  131.3 2.6 fusion
  133.9 33.9 %all-reduce = (f32[64,2,4]{2,1,0:T(2,128)S(1)}, f32[64,128]{1,0:T(8,128)S(1)}) all-reduce(f32[64,2,4]{2,1,0:T(2,128)S(1)} %fusion, f32[64,128]{1,0:T(8,128)S(1)} %fusion.17), channel_id=1, replica_groups=mesh['kv'=8,'tp'=4] {'kv'}, use_global_device_ids=true, to_apply=%region_11.12 | all-reduce | flops 8704 | bytes 69632 | tf_op jit(solution)/shard_map/psum | solution.py:73
  168.0 9.0 %fusion.2 = f32[64,2,4,64]{3,2,1,0:T(4,128)} fusion(bf16[64,2,64,1024]{3,2,1,0:T(8,128)(2,1)} %param.22, f32[64,2,4,1024]{3,2,1,0:T(4,128)S(1)} %copy-done.1, f32[64,2,4]{2,1,0:T(2,128)S(1)} %multiply_maximum_fusion), kind=kOutput, calls=%fused_computation.6 | convolution fusion | flops 68157440 | bytes 19007488 | tf_op jit(solution)/shard_map/bgjp,bgdp->bgjd/dot_general | solution.py:67
  177.2 69.7 %all-reduce.10.cloned.1.call-done = f32[64,2,4,64]{3,2,1,0:T(4,128)} async-done(((f32[64,2,4,64]{3,2,1,0:T(4,128)}), f32[64,2,4,64]{3,2,1,0:T(4,128)}) %all-reduce.10.cloned.1.call-update) | async-done | bytes 131088 | tf_op jit(solution)/shard_map/psum | solution.py:73
  246.9 1.3 fusion.7
  248.3 0.8 convolution_convert_fusion.1
  249.2 30.8 %all-reduce.12.cloned.1.call-done = bf16[64,512]{1,0:T(8,128)(2,1)} async-done(((bf16[64,512]{1,0:T(8,128)(2,1)}), bf16[64,512]{1,0:T(8,128)(2,1)}) %all-reduce.12.cloned.1.call-update) | async-done | bytes 65552 | tf_op jit(solution)/shard_map/psum | solution.py:81
  280.1 4.1 %fusion.14 = f32[64,4096]{1,0:T(8,128)} fusion(bf16[512,4096]{1,0:T(8,128)(2,1)} %param.26, f32[512]{0:T(512)S(1)} %copy-done.7, bf16[64,512]{1,0:T(8,128)(2,1)S(1)} %copy-done.2, bf16[64,512]{1,0:T(8,128)(2,1)} %all-reduce.12.cloned.1.call-done), kind=kOutput, calls=%fused_computation.26 | convolution fusion | flops 268664832 | bytes 5376000 | tf_op jit(solution)/shard_map/dot_general | solution.py:87
  284.4 21.7 %psum.85 = f32[64]{0:T(128)S(1)} all-reduce(f32[64]{0:T(128)S(1)} %fusion.11), channel_id=1, replica_groups=mesh['kv'=8,'tp'=4] {'kv'}, use_global_device_ids=true, to_apply=%region_14.15 | all-reduce | flops 64 | bytes 512 | tf_op jit(solution)/shard_map/psum | solution.py:88
  306.1 56.6 %all-reduce.14.cloned.1.call-done = f32[64,4096]{1,0:T(8,128)} async-done(((f32[64,4096]{1,0:T(8,128)}), f32[64,4096]{1,0:T(8,128)}) %all-reduce.14.cloned.1.call-update) | async-done | bytes 1048592 | tf_op jit(solution)/shard_map/psum | solution.py:88
  362.8 4.0 convolution_convert_fusion
  366.8 31.3 %all-reduce.16.cloned.1.call-done = bf16[64,512]{1,0:T(8,128)(2,1)} async-done(((bf16[64,512]{1,0:T(8,128)(2,1)}), bf16[64,512]{1,0:T(8,128)(2,1)}) %all-reduce.16.cloned.1.call-update) | async-done | bytes 65552 | tf_op jit(solution)/shard_map/psum | solution.py:92
  398.1 1.5 fusion.13
  (49 shorter events, 2.4 us)
Async XLA Ops:
  6.5 1.0 copy-start
  6.5 77.3 %all-reduce.8.cloned.1.call-start = ((), (), s32[]{:S(2)}) async-start(), calls=%async_computation | async-start | bytes 262144 | tf_op jit(solution)/shard_map/psum | solution.py:39
  9.3 237.6 %all-reduce.10.cloned.1.call-start = ((), (), s32[]{:S(2)}) async-start(), calls=%async_computation.1 | async-start | bytes 524288 | tf_op jit(solution)/shard_map/psum | solution.py:73
  51.9 2.2 copy-start.2
  51.9 2.2 copy-start.5
  51.9 2.2 copy-start.6
  51.9 33.5 %copy-start.8 = (f32[64]{0:T(128)S(1)}, f32[64]{0:T(128)}, u32[]{:S(2)}) copy-start(f32[64]{0:T(128)} %param.20) | copy-start | bytes 772
  95.1 72.8 %copy-start.1 = (f32[64,2,4,1024]{3,2,1,0:T(4,128)S(1)}, f32[64,2,4,1024]{3,2,1,0:T(4,128)}, u32[]{:S(2)}) copy-start(f32[64,2,4,1024]{3,2,1,0:T(4,128)} %get-tuple-element.15) | copy-start | bytes 6291460
  167.9 80.4 %copy-start.4 = (bf16[512,512]{1,0:T(8,128)(2,1)S(1)}, bf16[512,512]{1,0:T(8,128)(2,1)}, u32[]{:S(2)}) copy-start(bf16[512,512]{1,0:T(8,128)(2,1)} %param.24) | copy-start | bytes 1572868
  167.9 112.1 %copy-start.7 = (f32[512]{0:T(512)S(1)}, f32[512]{0:T(512)}, u32[]{:S(2)}) copy-start(f32[512]{0:T(512)} %param.25) | copy-start | bytes 6148
  176.9 103.1 %all-reduce.12.cloned.1.call-start = ((), (), s32[]{:S(2)}) async-start(), calls=%async_computation.2 | async-start | bytes 131072 | tf_op jit(solution)/shard_map/psum | solution.py:81
  249.2 113.6 %all-reduce.14.cloned.1.call-start = ((), (), s32[]{:S(2)}) async-start(), calls=%async_computation.3 | async-start | bytes 2097152 | tf_op jit(solution)/shard_map/psum | solution.py:88
  280.1 4.2 %copy-start.3 = (bf16[64,512]{1,0:T(8,128)(2,1)S(1)}, bf16[64,512]{1,0:T(8,128)(2,1)}, u32[]{:S(2)}) copy-start(bf16[64,512]{1,0:T(8,128)(2,1)} %all-reduce.12.cloned.1.call-done) | copy-start | bytes 196612
  284.2 113.9 %all-reduce.16.cloned.1.call-start = ((), (), s32[]{:S(2)}) async-start(), calls=%async_computation.4 | async-start | bytes 131072 | tf_op jit(solution)/shard_map/psum | solution.py:92
Sparse Core Ops, SparseCore 0:
  10.7 73.1 all-reduce.7
  177.1 69.7 all-reduce.9
  249.3 30.7 all-reduce.11
  284.4 78.3 all-reduce.13
  366.9 31.1 all-reduce.15
where the time goes:
time: 407 us; the launch traced here: 406 us
  waiting for transfers between devices  218 us (54%)
  blocking collectives  131 us (32%)
  matrix products  31.7 us (8%)
  between operations  13.4 us (3%)
  other arithmetic  8.11 us (2%)
    psum x1, waiting for transfers between devices, shards(): lax.psum((jnp.sum(weights, axis=-1), partial_values), 'kv')  69.7 us
    psum x1, waiting for transfers between devices, shards(): up_full, total_mlp = lax.psum((up_terms, squares_mlp), 'kv')  56.6 us
    psum x1, blocking collectives, shards(): lax.psum((query_terms, key_terms, value_terms, forget_terms, squares_mix)...  39.3 us
    pmax x1, blocking collectives, shards(): peak_score = jnp.maximum(lax.pmax(local_peak, 'kv'), own_score)  35.9 us
    psum x1, blocking collectives, shards(): lax.psum((jnp.sum(weights, axis=-1), partial_values), 'kv')  33.9 us
    psum x1, waiting for transfers between devices, shards(): mlp_out = lax.psum(down_terms.astype(jnp.bfloat16), 'tp')  31.3 us
    psum x1, waiting for transfers between devices, shards(): attn_out = lax.psum(attn_terms.astype(jnp.bfloat16), 'tp')  30.8 us
    psum x1, waiting for transfers between devices, shards(): lax.psum((query_terms, key_terms, value_terms, forget_terms, squares_mix)...  29.6 us
  transfers between devices with their start and end apart: 5, of which 5 were waited for; matrix products, arithmetic and copies ran while one was open for 1% of the time, Pallas kernels for 0%

commit v1 on v0

--- a/solution.py
+++ b/solution.py
@@ -89,7 +89,7 @@
     scale_mlp = lax.rsqrt(total_mlp / D + EPS)[:, None]
     hidden = jnp.square(jax.nn.relu(scale_mlp * up_full)).astype(jnp.bfloat16)
     down_terms = jnp.dot(hidden, w_down, preferred_element_type=jnp.float32)
-    mlp_out = lax.psum(down_terms.astype(jnp.bfloat16), "tp")
+    mlp_out = jnp.sum(lax.all_gather(down_terms.astype(jnp.bfloat16), "tp"), axis=0)
     mlp_rounded = lax.optimization_barrier(mlp_out).astype(jnp.float32)
     return (residual_wide + mlp_rounded).astype(jnp.bfloat16)
 

time: 407 us -> 380 us (0.934)
  waiting for transfers between devices: 218 us -> 187 us
  blocking collectives: 131 us -> 136 us
    psum x1 -> x0, waiting for transfers between devices: 31.3 us -> none  [shards(): mlp_out = lax.psum(down_terms.astype(jnp.bfloat16), 'tp')]
    all_gather x0 -> x1, blocking collectives: none -> 5.78 us  [shards(): lax.all_gather(down_terms.astype(jnp.bfloat16), 'tp')]
  transfers between devices with their start and end apart: 5 -> 4, of which waited for: 5 -> 4; matrix products, arithmetic and copies ran while one was open for 1% -> 2% of each run, Pallas kernels for 0% -> 0%
where the time goes in v1:
time: 380 us; the launch traced here: 379 us
  waiting for transfers between devices  187 us (49%)
  blocking collectives  136 us (36%)
  matrix products  31 us (8%)
  between operations  13.4 us (4%)
  other arithmetic  7.32 us (2%)
  local copies, waits for them, and re-layouts  3.95 us (1%)
    psum x1, waiting for transfers between devices, shards(): lax.psum((jnp.sum(weights, axis=-1), partial_values), 'kv')  69.7 us
    psum x1, waiting for transfers between devices, shards(): up_full, total_mlp = lax.psum((up_terms, squares_mlp), 'kv')  56.7 us
    psum x1, blocking collectives, shards(): lax.psum((query_terms, key_terms, value_terms, forget_terms, squares_mix)...  39.3 us
    pmax x1, blocking collectives, shards(): peak_score = jnp.maximum(lax.pmax(local_peak, 'kv'), own_score)  35.9 us
    psum x1, blocking collectives, shards(): lax.psum((jnp.sum(weights, axis=-1), partial_values), 'kv')  33.9 us
    psum x1, waiting for transfers between devices, shards(): attn_out = lax.psum(attn_terms.astype(jnp.bfloat16), 'tp')  30.8 us
    psum x1, waiting for transfers between devices, shards(): lax.psum((query_terms, key_terms, value_terms, forget_terms, squares_mix)...  29.6 us
    psum x1, blocking collectives, shards(): up_full, total_mlp = lax.psum((up_terms, squares_mlp), 'kv')  21.7 us
  transfers between devices with their start and end apart: 4, of which 4 were waited for; matrix products, arithmetic and copies ran while one was open for 2% of the time, Pallas kernels for 0%

profile of v1, /device:TPU:0, one launch (start us, length us, event | category | flops | bytes accessed | tf_op | source)
XLA Modules:
  0.0 379.2 jit_solution(14858623425260649025)
XLA Ops:
  6.5 1.0 copy-done
  7.6 1.7 fusion.23
  9.4 1.0 fusion.8
  10.3 1.1 fusion.19
  11.4 1.0 fusion.21
  12.4 39.3 %all-reduce.1 = (f32[64]{0:T(128)S(1)}, f32[64,8]{0,1:T(8,128)S(1)}, f32[64,128]{1,0:T(8,128)S(1)}) all-reduce(f32[64]{0:T(128)S(1)} %fusion.8, f32[64,8]{0,1:T(8,128)S(1)} %fusion.21, f32[64,128]{1,0:T(8,128)S(1)} %fusion.19), channel_id=1, replica_groups=mesh['kv'=8,'tp'=4] {'kv'}, use_global_device_ids=true, to_apply=%region_1.0 | all-reduce | flops 8768 | bytes 70144 | tf_op jit(solution)/shard_map/psum | solution.py:39
  51.9 2.0 reshape.49
  54.2 29.6 %all-reduce.7.cloned.1.call-done = f32[64,512]{1,0:T(8,128)} async-done(((f32[64,512]{1,0:T(8,128)}), f32[64,512]{1,0:T(8,128)}) %all-reduce.7.cloned.1.call-update) | async-done | bytes 131088 | tf_op jit(solution)/shard_map/psum | solution.py:39
  83.8 1.0 fusion.31
  85.7 9.4 %fusion.32 = (f32[64,2,4]{2,1,0:T(2,128)S(1)}, f32[64,2,4,1024]{3,2,1,0:T(4,128)}) fusion(f32[64,2,4]{2,1,0:T(2,128)S(1)} %copy.23, f32[64,2,4,1024]{3,2,1,0:T(4,128)S(1)} %reshape.49, bf16[64,2,4,64]{3,2,1,0:T(4,128)(2,1)S(1)} %multiply_convert_fusion.2, bf16[64,2,64,1024]{3,2,1,0:T(8,128)(2,1)} %param.21), kind=kOutput, calls=%fused_computation.47 | convolution fusion | flops 69205504 | bytes 21041152 | tf_op jit(solution)/shard_map/bgjd,bgdp->bgjp/dot_general | solution.py:56
  95.1 35.9 %pmax.7 = f32[64,2,4]{2,1,0:T(2,128)S(1)} all-reduce(f32[64,2,4]{2,1,0:T(2,128)S(1)} %get-tuple-element.14), channel_id=1, replica_groups=mesh['kv'=8,'tp'=4] {'kv'}, use_global_device_ids=true, to_apply=%region_6.0 | all-reduce | flops 512 | bytes 4096 | tf_op jit(solution)/shard_map/pmax | solution.py:65
  131.3 2.6 fusion
  133.9 33.9 %all-reduce = (f32[64,2,4]{2,1,0:T(2,128)S(1)}, f32[64,128]{1,0:T(8,128)S(1)}) all-reduce(f32[64,2,4]{2,1,0:T(2,128)S(1)} %fusion, f32[64,128]{1,0:T(8,128)S(1)} %fusion.17), channel_id=1, replica_groups=mesh['kv'=8,'tp'=4] {'kv'}, use_global_device_ids=true, to_apply=%region_11.12 | all-reduce | flops 8704 | bytes 69632 | tf_op jit(solution)/shard_map/psum | solution.py:73
  168.0 9.0 %fusion.2 = f32[64,2,4,64]{3,2,1,0:T(4,128)} fusion(bf16[64,2,64,1024]{3,2,1,0:T(8,128)(2,1)} %param.22, f32[64,2,4,1024]{3,2,1,0:T(4,128)S(1)} %copy-done.1, f32[64,2,4]{2,1,0:T(2,128)S(1)} %multiply_maximum_fusion), kind=kOutput, calls=%fused_computation.6 | convolution fusion | flops 68157440 | bytes 19007488 | tf_op jit(solution)/shard_map/bgjp,bgdp->bgjd/dot_general | solution.py:67
  177.2 69.7 %all-reduce.9.cloned.1.call-done = f32[64,2,4,64]{3,2,1,0:T(4,128)} async-done(((f32[64,2,4,64]{3,2,1,0:T(4,128)}), f32[64,2,4,64]{3,2,1,0:T(4,128)}) %all-reduce.9.cloned.1.call-update) | async-done | bytes 131088 | tf_op jit(solution)/shard_map/psum | solution.py:73
  246.9 1.3 fusion.7
  248.3 0.8 convolution_convert_fusion.1
  249.2 30.8 %all-reduce.11.cloned.1.call-done = bf16[64,512]{1,0:T(8,128)(2,1)} async-done(((bf16[64,512]{1,0:T(8,128)(2,1)}), bf16[64,512]{1,0:T(8,128)(2,1)}) %all-reduce.11.cloned.1.call-update) | async-done | bytes 65552 | tf_op jit(solution)/shard_map/psum | solution.py:81
  280.1 4.1 %fusion.14 = f32[64,4096]{1,0:T(8,128)} fusion(bf16[512,4096]{1,0:T(8,128)(2,1)} %param.26, f32[512]{0:T(512)S(1)} %copy-done.7, bf16[64,512]{1,0:T(8,128)(2,1)S(1)} %copy-done.2, bf16[64,512]{1,0:T(8,128)(2,1)} %all-reduce.11.cloned.1.call-done), kind=kOutput, calls=%fused_computation.26 | convolution fusion | flops 268664832 | bytes 5376000 | tf_op jit(solution)/shard_map/dot_general | solution.py:87
  284.4 21.7 %psum.78 = f32[64]{0:T(128)S(1)} all-reduce(f32[64]{0:T(128)S(1)} %fusion.11), channel_id=1, replica_groups=mesh['kv'=8,'tp'=4] {'kv'}, use_global_device_ids=true, to_apply=%region_14.15 | all-reduce | flops 64 | bytes 512 | tf_op jit(solution)/shard_map/psum | solution.py:88
  306.1 56.7 %all-reduce.13.cloned.1.call-done = f32[64,4096]{1,0:T(8,128)} async-done(((f32[64,4096]{1,0:T(8,128)}), f32[64,4096]{1,0:T(8,128)}) %all-reduce.13.cloned.1.call-update) | async-done | bytes 1048592 | tf_op jit(solution)/shard_map/psum | solution.py:88
  362.7 3.4 convolution_convert_fusion
  366.1 5.8 %all-gather = bf16[256,512]{1,0:T(8,128)(2,1)S(1)} all-gather(bf16[64,512]{1,0:T(8,128)(2,1)S(1)} %convolution_convert_fusion), channel_id=2, replica_groups=mesh['kv'=8,'tp'=4] {'tp'}, dimensions={0}, use_global_device_ids=true | all-gather | bytes 327680 | tf_op jit(solution)/shard_map/all_gather | solution.py:92
  372.0 0.7 fusion.13
  (48 shorter events, 2.4 us)
Async XLA Ops:
  6.5 1.0 copy-start
  6.5 77.3 %all-reduce.7.cloned.1.call-start = ((), (), s32[]{:S(2)}) async-start(), calls=%async_computation | async-start | bytes 262144 | tf_op jit(solution)/shard_map/psum | solution.py:39
  9.3 237.6 %all-reduce.9.cloned.1.call-start = ((), (), s32[]{:S(2)}) async-start(), calls=%async_computation.1 | async-start | bytes 524288 | tf_op jit(solution)/shard_map/psum | solution.py:73
  51.9 2.2 copy-start.2
  51.9 2.2 copy-start.5
  51.9 2.2 copy-start.6
  51.9 33.5 %copy-start.8 = (f32[64]{0:T(128)S(1)}, f32[64]{0:T(128)}, u32[]{:S(2)}) copy-start(f32[64]{0:T(128)} %param.20) | copy-start | bytes 772
  95.1 72.8 %copy-start.1 = (f32[64,2,4,1024]{3,2,1,0:T(4,128)S(1)}, f32[64,2,4,1024]{3,2,1,0:T(4,128)}, u32[]{:S(2)}) copy-start(f32[64,2,4,1024]{3,2,1,0:T(4,128)} %get-tuple-element.15) | copy-start | bytes 6291460
  167.9 80.4 %copy-start.4 = (bf16[512,512]{1,0:T(8,128)(2,1)S(1)}, bf16[512,512]{1,0:T(8,128)(2,1)}, u32[]{:S(2)}) copy-start(bf16[512,512]{1,0:T(8,128)(2,1)} %param.24) | copy-start | bytes 1572868
  167.9 112.1 %copy-start.7 = (f32[512]{0:T(512)S(1)}, f32[512]{0:T(512)}, u32[]{:S(2)}) copy-start(f32[512]{0:T(512)} %param.25) | copy-start | bytes 6148
  176.9 103.1 %all-reduce.11.cloned.1.call-start = ((), (), s32[]{:S(2)}) async-start(), calls=%async_computation.2 | async-start | bytes 131072 | tf_op jit(solution)/shard_map/psum | solution.py:81
  249.2 113.5 %all-reduce.13.cloned.1.call-start = ((), (), s32[]{:S(2)}) async-start(), calls=%async_computation.3 | async-start | bytes 2097152 | tf_op jit(solution)/shard_map/psum | solution.py:88
  280.1 4.2 %copy-start.3 = (bf16[64,512]{1,0:T(8,128)(2,1)S(1)}, bf16[64,512]{1,0:T(8,128)(2,1)}, u32[]{:S(2)}) copy-start(bf16[64,512]{1,0:T(8,128)(2,1)} %all-reduce.11.cloned.1.call-done) | copy-start | bytes 196612
Sparse Core Ops, SparseCore 0:
  10.7 73.1 all-reduce.6
  177.1 69.7 all-reduce.8
  249.3 30.7 all-reduce.10
  284.4 78.3 all-reduce.12
